TPU v7x, 32 devices: a whole 2x2x4 slice. The times are simulated.
32 devices in a mesh: sp: 8 (over z, x), tp: 4 (over y, core).
Axes of the slice: x: 2, y: 2, z: 4, core: 2. Of those that a mesh axis runs over, the one named last changes fastest.
Arguments:
- tokens: bfloat16 [8, 80, 4096], P(None, 'sp', 'tp'), may hold values from -6 to 6
- latent_down_weight: bfloat16 [4096, 512], replicated, may hold values from -0.09375 to 0.09375
- w_rope_key: bfloat16 [4096, 64], replicated, may hold values from -0.09375 to 0.09375
- latent_norm_gain: float32 [512], replicated, may hold values from 0.1 to 1.9
- key_up_weight: bfloat16 [512, 4096], P(None, 'tp'), may hold values from -0.25 to 0.25
- value_up_weight: bfloat16 [512, 4096], P(None, 'tp'), may hold values from -0.25 to 0.25
- cached_latent_rows: bfloat16 [8, 32768, 512], P('sp', 'tp'), may hold values from -6 to 6
- past_rope: bfloat16 [8, 32768, 64], P('sp', 'tp'), may hold values from -6 to 6
- query_nope: bfloat16 [8, 4096], P('sp', 'tp'), may hold values from -8 to 8
- query_rope: bfloat16 [8, 2048], P('sp', 'tp'), may hold values from -300 to 300
Outputs:
- new_keys: bfloat16 [8, 80, 4096], P('sp', None, 'tp')
- new_values: bfloat16 [8, 80, 4096], P('sp', None, 'tp')
- new_rope: bfloat16 [8, 80, 64], P('sp')
- attended: bfloat16 [8, 4096], P('sp', 'tp')
All inputs are finite; a program needn't handle non-finite values.
Results may differ from a plain program's by a relative error of at most 0.0085.
Values may be sent and summed in bfloat16 or wider, within the bound.
A program may use at most 64 MiB of HBM per device.

v0:
```python
import jax
import jax.numpy as jnp
from jax import lax
from jax.sharding import PartitionSpec as P

PLAIN_KEY_WIDTH = 128
ROPE = 64
VALUE_WIDTH = 128
PAST_POSITIONS = 32768
epsilon = 1e-06
rope_theta = 10000.0


def combined_all(part, axis, combine):
    gathered = jax.tree.map(lambda a: lax.all_gather(a, axis), part)

    def take(source):
        return jax.tree.map(lambda a: lax.dynamic_index_in_dim(a, source, 0, False), gathered)

    return lax.fori_loop(
        1, lax.axis_size(axis), lambda source, state: combine(state, take(source)), take(0)
    )


def rotate(values, positions):
    halfway = values.shape[-1] // 2
    frequency = rope_theta ** (-jnp.arange(halfway, dtype=jnp.float32) / halfway)
    angles = positions[:, None] * frequency
    first = values[..., :halfway]
    second = values[..., halfway:]
    return jnp.concatenate(
        [
            first * jnp.cos(angles) - second * jnp.sin(angles),
            first * jnp.sin(angles) + second * jnp.cos(angles),
        ],
        axis=-1,
    )


def combine_parts(first, second):
    highest = jnp.maximum(first[0], second[0])
    scale_first = jnp.exp(first[0] - highest)
    scale_second = jnp.exp(second[0] - highest)
    total = first[1] * scale_first + second[1] * scale_second
    summed = first[2] * scale_first[..., None] + second[2] * scale_second[..., None]
    return (highest, total, summed)


def on_device(
    tokens,
    latent_down_weight,
    w_rope_key,
    latent_norm_gain,
    key_up_weight,
    value_up_weight,
    cached_latent_rows,
    past_rope,
    query_nope,
    query_rope,
):
    rows_here = lax.all_to_all(tokens, "sp", split_axis=0, concat_axis=1, tiled=True)
    prompts, per_seq, features = rows_here.shape
    row_count = prompts * per_seq
    latent_width = latent_down_weight.shape[1]
    turn_width = w_rope_key.shape[1]
    factor = (PLAIN_KEY_WIDTH + ROPE) ** (-0.5)
    fragment = lax.all_gather(rows_here, "tp", axis=2, tiled=True)
    columns = fragment.shape[2]
    flat_rows = fragment.reshape(row_count, columns)
    latent_raw = jnp.dot(flat_rows, latent_down_weight, preferred_element_type=jnp.float32)
    rope_raw = jnp.dot(flat_rows, w_rope_key, preferred_element_type=jnp.float32)
    scale = lax.rsqrt(jnp.mean(latent_raw * latent_raw, axis=-1, keepdims=True) + epsilon)
    latent = (latent_raw * scale * latent_norm_gain).astype(jnp.bfloat16)
    positions = (PAST_POSITIONS + jnp.arange(per_seq)).astype(jnp.float32)
    rope_local = rotate(rope_raw.reshape(prompts, per_seq, turn_width), positions).astype(
        jnp.bfloat16
    )
    keys_local = (
        jnp.dot(latent, key_up_weight, preferred_element_type=jnp.float32)
        .astype(jnp.bfloat16)
        .reshape(prompts, per_seq, key_up_weight.shape[1])
    )
    values_local = (
        jnp.dot(latent, value_up_weight, preferred_element_type=jnp.float32)
        .astype(jnp.bfloat16)
        .reshape(prompts, per_seq, value_up_weight.shape[1])
    )
    new_keys, new_values, new_rope = (keys_local, values_local, rope_local)
    owned = query_nope.shape[0]
    heads_local = query_nope.shape[1] // PLAIN_KEY_WIDTH
    query_own = query_nope.reshape(owned, heads_local, PLAIN_KEY_WIDTH)
    turn_own = query_rope.reshape(owned, heads_local, ROPE)
    head_keys = key_up_weight.reshape(latent_width, heads_local, PLAIN_KEY_WIDTH)
    query_latent = jnp.einsum(
        "shd,khd->shk", query_own, head_keys, preferred_element_type=jnp.float32
    ).astype(jnp.bfloat16)
    every_latent, every_turn = (
        lax.all_gather(query_latent, "tp", axis=1, tiled=True),
        lax.all_gather(turn_own, "tp", axis=1, tiled=True),
    )
    past_scores = jnp.einsum(
        "shk,spk->shp", every_latent, cached_latent_rows, preferred_element_type=jnp.float32
    )
    past_scores = (
        past_scores
        + jnp.einsum("shd,spd->shp", every_turn, past_rope, preferred_element_type=jnp.float32)
    ) * factor
    local_peak = jnp.max(past_scores, axis=-1)
    local_weight = jnp.exp(past_scores - local_peak[:, :, None])
    local_total = jnp.sum(local_weight, axis=-1)
    local_latent = jnp.einsum(
        "shp,spk->shk",
        local_weight.astype(jnp.bfloat16),
        cached_latent_rows,
        preferred_element_type=jnp.float32,
    )
    peak_all, total_all, latent_all = combined_all(
        (local_peak, local_total, local_latent), "tp", combine_parts
    )
    start = lax.axis_index("tp") * heads_local
    past_peak = lax.dynamic_slice_in_dim(peak_all, start, heads_local, 1)
    past_total = lax.dynamic_slice_in_dim(total_all, start, heads_local, 1)
    past_sum = lax.dynamic_slice_in_dim(latent_all, start, heads_local, 1)
    fresh = new_keys.shape[1]
    new_scores = jnp.einsum(
        "shd,sphd->shp",
        query_own,
        new_keys.reshape(owned, fresh, heads_local, PLAIN_KEY_WIDTH),
        preferred_element_type=jnp.float32,
    )
    new_scores = (
        new_scores
        + jnp.einsum("shd,spd->shp", turn_own, new_rope, preferred_element_type=jnp.float32)
    ) * factor
    peak = jnp.maximum(past_peak, jnp.max(new_scores, axis=-1))
    past_share = jnp.exp(past_peak - peak)
    new_weight = jnp.exp(new_scores - peak[:, :, None])
    denominator = past_total * past_share + jnp.sum(new_weight, axis=-1)
    latent_sum = (past_sum * past_share[..., None]).astype(jnp.bfloat16)
    head_values = value_up_weight.reshape(latent_width, heads_local, VALUE_WIDTH)
    past_out = jnp.einsum(
        "shk,khd->shd", latent_sum, head_values, preferred_element_type=jnp.float32
    )
    new_out = jnp.einsum(
        "shp,sphd->shd",
        new_weight.astype(jnp.bfloat16),
        new_values.reshape(owned, fresh, heads_local, VALUE_WIDTH),
        preferred_element_type=jnp.float32,
    )
    attended = (
        ((past_out + new_out) / denominator[:, :, None])
        .astype(jnp.bfloat16)
        .reshape(owned, heads_local * VALUE_WIDTH)
    )
    return (new_keys, new_values, new_rope, attended)


def solution(mesh):
    in_specs = (
        P(None, "sp", "tp"),
        P(),
        P(),
        P(),
        P(None, "tp"),
        P(None, "tp"),
        P("sp", "tp", None),
        P("sp", "tp", None),
        P("sp", "tp"),
        P("sp", "tp"),
    )
    out_specs = (P("sp", None, "tp"), P("sp", None, "tp"), P("sp", None, None), P("sp", "tp"))
    return jax.shard_map(
        on_device, mesh=mesh, in_specs=in_specs, out_specs=out_specs, check_vma=False
    )
```

profile of v0, /device:TPU:0, one launch (start us, length us, event | category | flops | bytes accessed | tf_op | source)
XLA Modules:
  0.0 66.8 jit_solution(9695988542635753334)
XLA Ops:
  0.6 1.8 %copy.21 = bf16[8,10,1024]{2,1,0:T(8,128)(2,1)} copy(bf16[8,10,1024]{2,0,1:T(8,128)(2,1)} %param.12) | data formatting | bytes 327680 | tf_op args[0]
  2.4 7.3 %all-to-all-start = ((bf16[8,10,1024]{2,1,0:T(8,128)(2,1)}), bf16[8,10,1024]{2,1,0:T(8,128)(2,1)}, u32[]{:S(2)}, u32[]{:S(2)}) async-start(bf16[8,10,1024]{2,1,0:T(8,128)(2,1)} %copy.21), calls=%async_computation | async-start | bytes 524288 | tf_op jit(solution)/shard_map/all_to_all | solution.py:61
  9.7 0.7 %reduce.8 = bf16[512]{0:T(512)(128)(2,1)S(1)} reduce(bf16[1,512]{1,0:T(2,128)(2,1)} %param.21, bf16[]{:T(256)} %constant.97), dimensions={0}, to_apply=%param.21.reduce_sub_computation | reduce | bytes 2050 | tf_op args[9]
  10.5 5.2 %all_gather.29 = bf16[1,32,64]{2,1,0:T(8,128)(2,1)S(1)} all-gather(bf16[1,8,64]{2,1,0:T(8,128)(2,1)S(1)} %reshape.326), channel_id=1, replica_groups=mesh['sp'=8,'tp'=4] {'tp'}, dimensions={1}, use_global_device_ids=true | all-gather | bytes 5120 | tf_op jit(solution)/shard_map/all_gather | solution.py:99
  15.7 1.6 %fusion.18 = bf16[8,1,512]{2,1,0:T(2,128)(2,1)S(1)} fusion(bf16[1,1024]{1,0:T(2,128)(2,1)} %param.20, bf16[512,1024]{1,0:T(8,128)(2,1)} %param.16), kind=kOutput, calls=%fused_computation.28 | convolution fusion | flops 1048576 | bytes 1058816 | tf_op jit(solution)/shard_map/shd,khd->shk/dot_general | solution.py:94
  17.3 5.2 %all-gather = bf16[32,512]{1,0:T(8,128)(2,1)S(1)} all-gather(bf16[8,512]{1,0:T(8,128)(2,1)S(1)} %bitcast.161), channel_id=2, replica_groups=mesh['sp'=8,'tp'=4] {'tp'}, dimensions={0}, use_global_device_ids=true | all-gather | bytes 40960 | tf_op jit(solution)/shard_map/all_gather | solution.py:98
  22.5 5.9 %fusion.11 = f32[32,8192]{1,0:T(8,128)S(1)} fusion(bf16[32,512]{1,0:T(8,128)(2,1)S(1)} %all-gather, bf16[1,8192,512]{2,1,0:T(8,128)(2,1)} %param.18), kind=kOutput, calls=%fused_computation.17 | convolution fusion | flops 268435456 | bytes 9469952 | tf_op jit(solution)/shard_map/shk,spk->shp/dot_general | solution.py:101
  28.4 0.4 fusion.64
  28.8 0.4 fusion.23
  29.2 0.6 dynamic-slice
  30.5 0.2 dynamic-update-slice
  30.9 7.1 %all-reduce.2 = (f32[128]{0:T(128)S(1)}, f32[128]{0:T(128)S(1)}) all-reduce(f32[128]{0:T(128)S(1)} %dynamic-update-slice, f32[128]{0:T(128)S(1)} %dynamic-update-slice.1), channel_id=3, replica_groups=mesh['sp'=8,'tp'=4] {'tp'}, use_global_device_ids=true, to_apply=%add | all-reduce | flops 256 | bytes 2048
  38.2 5.1 %fusion.9 = f32[32,512]{1,0:T(8,128)S(1)} fusion(bf16[1,8192,512]{2,1,0:T(8,128)(2,1)} %param.18, f32[32,8192]{1,0:T(8,128)S(1)} %get-tuple-element.237, f32[32]{0:T(128)S(1)} %get-tuple-element.236), kind=kOutput, calls=%fused_computation.15 | convolution fusion | flops 268959744 | bytes 9502848 | tf_op jit(solution)/shard_map/shp,spk->shk/dot_general | solution.py:111
  43.2 5.9 %all-gather.3 = f32[128,512]{1,0:T(8,128)S(1)} all-gather(f32[32,512]{1,0:T(8,128)S(1)} %fusion.9), channel_id=5, replica_groups=mesh['sp'=8,'tp'=4] {'tp'}, dimensions={0}, use_global_device_ids=true | all-gather | bytes 327680 | tf_op jit(solution)/shard_map/all_gather | solution.py:15
  49.2 0.5 while.19
  49.7 1.0 %all_to_all.10 = bf16[1,80,1024]{2,1,0:T(8,128)(2,1)S(1)} reshape(bf16[8,10,1024]{2,1,0:T(8,128)(2,1)} %all-to-all-done) | data formatting | bytes 327680 | tf_op jit(solution)/shard_map/all_to_all | solution.py:61
  50.7 8.0 %all_gather.27 = bf16[1,80,4096]{2,1,0:T(8,128)(2,1)S(1)} all-gather(bf16[1,80,1024]{2,1,0:T(8,128)(2,1)S(1)} %all_to_all.10), channel_id=1, replica_groups=mesh['sp'=8,'tp'=4] {'tp'}, dimensions={2}, use_global_device_ids=true | all-gather | bytes 819200 | tf_op jit(solution)/shard_map/all_gather | solution.py:67
  58.7 3.1 %multiply_reduce_fusion = (f32[80]{0:T(128)S(1)}, f32[80,512]{1,0:T(8,128)S(1)}) fusion(bf16[4096,512]{1,0:T(8,128)(2,1)} %param.13, bf16[1,80,4096]{2,1,0:T(8,128)(2,1)S(1)} %all_gather.27), kind=kOutput, calls=%fused_computation.46 | convolution fusion | flops 335626176 | bytes 5013824 | tf_op jit(solution)/shard_map/dot_general | solution.py:70
  61.9 0.4 convolution_convert_fusion.1
  62.5 1.4 %convolution_bitcast_fusion = f32[1,80,64]{1,2,0:T(8,128)S(1)} fusion(bf16[4096,64]{0,1:T(8,128)(2,1)} %param.14, bf16[1,80,4096]{2,1,0:T(8,128)(2,1)S(1)} %all_gather.27), kind=kOutput, calls=%fused_computation.21 | convolution fusion | flops 41943040 | bytes 1200128 | tf_op jit(solution)/shard_map/dot_general | solution.py:71
  63.9 0.4 convolution_convert_fusion
  64.4 0.6 pad_maximum_fusion
  65.7 0.3 fusion.15
  66.2 0.6 copy.64
  (51 shorter events, 2.2 us)
Async XLA Ops:
  0.6 27.8 %copy-start = (bf16[1,8192,64]{1,2,0:T(8,128)(2,1)S(1)}, bf16[1,8192,64]{1,2,0:T(8,128)(2,1)}, u32[]{:S(2)}) copy-start(bf16[1,8192,64]{1,2,0:T(8,128)(2,1)} %param.19) | copy-start | bytes 3145732
  2.4 47.3 %all-to-all-start = ((bf16[8,10,1024]{2,1,0:T(8,128)(2,1)}), bf16[8,10,1024]{2,1,0:T(8,128)(2,1)}, u32[]{:S(2)}, u32[]{:S(2)}) async-start(bf16[8,10,1024]{2,1,0:T(8,128)(2,1)} %copy.21), calls=%async_computation | async-start | bytes 524288 | tf_op jit(solution)/shard_map/all_to_all | solution.py:61
  22.5 6.7 %copy-start.7 = (u32[32]{0:T(128)S(1)}, u32[32]{0:T(128)}, u32[]{:S(2)}) copy-start(u32[32]{0:T(128)} %constant.87) | copy-start | bytes 388
  38.2 23.7 %copy-start.1 = (bf16[512,1024]{1,0:T(8,128)(2,1)S(1)}, bf16[512,1024]{1,0:T(8,128)(2,1)}, u32[]{:S(2)}) copy-start(bf16[512,1024]{1,0:T(8,128)(2,1)} %param.16) | copy-start | bytes 3145732
  38.2 23.7 %copy-start.5 = (f32[512]{0:T(512)S(1)}, f32[512]{0:T(512)}, u32[]{:S(2)}) copy-start(f32[512]{0:T(512)} %param.15) | copy-start | bytes 6148
  43.2 19.0 %copy-start.6 = (bf16[1,1024]{1,0:T(2,128)(2,1)S(1)}, bf16[1,1024]{1,0:T(2,128)(2,1)}, u32[]{:S(2)}) copy-start(bf16[1,1024]{1,0:T(2,128)(2,1)} %param.20) | copy-start | bytes 6148
  43.2 20.7 %copy-start.2 = (bf16[512,1024]{1,0:T(8,128)(2,1)S(1)}, bf16[512,1024]{1,0:T(8,128)(2,1)}, u32[]{:S(2)}) copy-start(bf16[512,1024]{1,0:T(8,128)(2,1)} %param.17) | copy-start | bytes 3145732
  62.3 4.5 %copy-start.3 = (bf16[80,1024]{1,0:T(8,128)(2,1)}, bf16[80,1024]{1,0:T(8,128)(2,1)S(1)}, u32[]{:S(2)}) copy-start(bf16[80,1024]{1,0:T(8,128)(2,1)S(1)} %convolution_convert_fusion.1) | copy-start | bytes 491524
  64.3 2.6 %copy-start.4 = (bf16[80,1024]{1,0:T(8,128)(2,1)}, bf16[80,1024]{1,0:T(8,128)(2,1)S(1)}, u32[]{:S(2)}) copy-start(bf16[80,1024]{1,0:T(8,128)(2,1)S(1)} %convolution_convert_fusion) | copy-start | bytes 491524
where the time goes:
time: 67.3 us; the launch traced here: 66.8 us
  blocking collectives  31.4 us (47%)
  matrix products  19.1 us (28%)
  starting transfers between devices  7.28 us (11%)
  local copies, waits for them, and re-layouts  4.87 us (7%)
  other arithmetic  2.69 us (4%)
  between operations  1.45 us (2%)
    all_gather x1, blocking collectives, on_device(): fragment = lax.all_gather(rows_here, 'tp', axis=2, tiled=True)  7.99 us
    all_to_all x1, starting transfers between devices, on_device(): lax.all_to_all(tokens, 'sp', split_axis=0, concat_axis=1, tiled=True)  7.28 us
    unnamed x1, blocking collectives  7.09 us
    dot_general x1, matrix products, on_device(): jnp.einsum('shk,spk->shp', every_latent, cached_latent_rows, preferred_el...  5.92 us
    all_gather x1, blocking collectives, combined_all(): gathered = jax.tree.map(lambda a: lax.all_gather(a, axis), part)  5.91 us
    all_gather x1, blocking collectives, on_device(): lax.all_gather(query_latent, 'tp', axis=1, tiled=True)  5.19 us
    all_gather x1, blocking collectives, on_device(): lax.all_gather(turn_own, 'tp', axis=1, tiled=True)  5.18 us
    dot_general x1, matrix products, on_device(): jnp.einsum('shp,spk->shk', local_weight.astype(jnp.bfloat16), cached_late...  5.06 us
  transfers between devices with their start and end apart: 1, of which 0 were waited for; matrix products, arithmetic and copies ran while one was open for 24% of the time, Pallas kernels for 0%

commit v1 on v0

--- a/solution.py
+++ b/solution.py
@@ -9,6 +9,17 @@
 PAST_POSITIONS = 32768
 epsilon = 1e-06
 rope_theta = 10000.0
+
+
+def split_up(array, dim, devices):
+    before, after = (array.shape[:dim], array.shape[dim + 1 :])
+    return jnp.moveaxis(array.reshape(*before, devices, -1, *after), dim, 0)
+
+
+def in_order(blocks, dim):
+    blocks = jnp.moveaxis(blocks, 0, dim)
+    shape = blocks.shape
+    return blocks.reshape(*shape[:dim], shape[dim] * shape[dim + 1], *shape[dim + 2 :])
 
 
 def combined_all(part, axis, combine):
@@ -58,7 +69,14 @@
     query_nope,
     query_rope,
 ):
-    rows_here = lax.all_to_all(tokens, "sp", split_axis=0, concat_axis=1, tiled=True)
+    devices, index = (lax.axis_size("sp"), lax.axis_index("sp"))
+    blocks = split_up(tokens, 0, devices)
+    outs = [blocks[index]]
+    for turn in range(1, devices):
+        sent = blocks[(index + turn) % devices]
+        outs.append(lax.ppermute(sent, "sp", [(i, (i + turn) % devices) for i in range(devices)]))
+    blocks = jnp.stack(outs)[(index - jnp.arange(devices)) % devices]
+    rows_here = in_order(blocks, 1)
     prompts, per_seq, features = rows_here.shape
     row_count = prompts * per_seq
     latent_width = latent_down_weight.shape[1]

time: 67.3 us -> 96.7 us (1.44)
  local copies, waits for them, and re-layouts: 4.87 us -> 23.6 us
  other arithmetic: 2.69 us -> 10.1 us
  starting transfers between devices: 7.28 us -> 13.8 us
  matrix products: 19.1 us -> 15.9 us
    ppermute x0 -> x7, starting transfers between devices: none -> 13.8 us  [on_device(): lax.ppermute(sent, 'sp', [(i, (i + turn) % devices) for i in range(device...]
    unnamed x23 -> x52, local copies, waits for them, and re-layouts: 3.5 us -> 13.5 us
    all_to_all x1 -> x0, starting transfers between devices: 7.28 us -> none  [on_device(): lax.all_to_all(tokens, 'sp', split_axis=0, concat_axis=1, tiled=True)]
    exp x3, other arithmetic: 0.07 us -> 3.78 us  [combine_parts(): scale_second = jnp.exp(second[0] - highest)]
    dot_general x1, matrix products: 5.06 us -> 1.62 us  [on_device(): jnp.einsum('shp,spk->shk', local_weight.astype(jnp.bfloat16), cached_late...]
    another operation x1 -> x3, local copies, waits for them, and re-layouts: 0.08 us -> 2.66 us
    squeeze x0 -> x1, local copies, waits for them, and re-layouts: none -> 2.24 us  [on_device(): sent = blocks[(index + turn) % devices]]
    mul x3, other arithmetic: 0.03 us -> 2 us  [combine_parts(): first[2] * scale_first[..., None] + second[2] * scale_second[..., None]]
  transfers between devices with their start and end apart: 1 -> 7, of which waited for: 0 -> 0; matrix products, arithmetic and copies ran while one was open for 24% -> 37% of each run, Pallas kernels for 0% -> 0%
where the time goes in v1:
time: 96.7 us; the launch traced here: 96 us
  blocking collectives  30.8 us (32%)
  local copies, waits for them, and re-layouts  23.6 us (24%)
  matrix products  15.9 us (16%)
  starting transfers between devices  13.8 us (14%)
  other arithmetic  10.1 us (10%)
  between operations  1.72 us (2%)
    ppermute x7, starting transfers between devices, on_device(): lax.ppermute(sent, 'sp', [(i, (i + turn) % devices) for i in range(device...  13.8 us
    unnamed x52, local copies, waits for them, and re-layouts  13.5 us
    all_gather x1, blocking collectives, on_device(): fragment = lax.all_gather(rows_here, 'tp', axis=2, tiled=True)  7.63 us
    unnamed x1, blocking collectives  7.09 us
    dot_general x1, matrix products, on_device(): jnp.einsum('shk,spk->shp', every_latent, cached_latent_rows, preferred_el...  6.05 us
    all_gather x1, blocking collectives, combined_all(): gathered = jax.tree.map(lambda a: lax.all_gather(a, axis), part)  5.76 us
    all_gather x1, blocking collectives, on_device(): lax.all_gather(query_latent, 'tp', axis=1, tiled=True)  5.19 us
    all_gather x1, blocking collectives, on_device(): lax.all_gather(turn_own, 'tp', axis=1, tiled=True)  5.18 us
  transfers between devices with their start and end apart: 7, of which 0 were waited for; matrix products, arithmetic and copies ran while one was open for 37% of the time, Pallas kernels for 0%

profile of v1, /device:TPU:0, one launch (start us, length us, event | category | flops | bytes accessed | tf_op | source)
XLA Modules:
  0.0 96.0 jit_solution(8943003938503257793)
XLA Ops:
  0.7 2.2 %constant_dynamic-slice_fusion.4 = (bf16[1,10,1024]{2,0,1:T(2,128)(2,1)S(1)}, bf16[1,10,1024]{2,0,1:T(2,128)(2,1)S(1)}, bf16[1,10,1024]{2,0,1:T(2,128)(2,1)S(1)}...) fusion(bf16[8,10,1024]{2,0,1:T(8,128)(2,1)} %param.12, ...), kind=kLoop, calls=%fused_computation.89 | loop fusion | bytes 327712 | tf_op jit(solution)/shard_map/squeeze | solution.py:76
  3.6 3.0 %collective-permute-start = (bf16[1,10,1024]{2,1,0:T(8,128)(2,1)}, bf16[1,10,1024]{2,1,0:T(8,128)(2,1)}, u32[]{:S(2)}, u32[]{:S(2)}) collective-permute-start(bf16[1,10,1024]{2,1,0:T(8,128)(2,1)} %copy.46), channel_id=1, source_target_pairs={{0,4},{4,8},{8,12},{12,16},{16,20},{20,24},{24,28},{28,0},{1,5},{5... | collective-permute-start | bytes 61448 | tf_op jit(solution)/shard_map/ppermute | solution.py:77
  7.2 1.6 %collective-permute-start.1 = (bf16[1,10,1024]{2,1,0:T(8,128)(2,1)}, bf16[1,10,1024]{2,1,0:T(8,128)(2,1)}, u32[]{:S(2)}, u32[]{:S(2)}) collective-permute-start(bf16[1,10,1024]{2,1,0:T(8,128)(2,1)} %copy.47), channel_id=1, source_target_pairs={{0,8},{4,12},{8,16},{12,20},{16,24},{20,28},{24,0},{28,4},{1,9},{5... | collective-permute-start | bytes 61448 | tf_op jit(solution)/shard_map/ppermute | solution.py:77
  9.4 2.6 %collective-permute-start.2 = (bf16[1,10,1024]{2,1,0:T(8,128)(2,1)}, bf16[1,10,1024]{2,1,0:T(8,128)(2,1)}, u32[]{:S(2)}, u32[]{:S(2)}) collective-permute-start(bf16[1,10,1024]{2,1,0:T(8,128)(2,1)} %copy.48), channel_id=1, source_target_pairs={{0,12},{4,16},{8,20},{12,24},{16,28},{20,0},{24,4},{28,8},{1,13},{... | collective-permute-start | bytes 61448 | tf_op jit(solution)/shard_map/ppermute | solution.py:77
  14.4 2.6 %collective-permute-start.4 = (bf16[1,10,1024]{2,1,0:T(8,128)(2,1)}, bf16[1,10,1024]{2,1,0:T(8,128)(2,1)}, u32[]{:S(2)}, u32[]{:S(2)}) collective-permute-start(bf16[1,10,1024]{2,1,0:T(8,128)(2,1)} %copy.50), channel_id=1, source_target_pairs={{0,20},{4,24},{8,28},{12,0},{16,4},{20,8},{24,12},{28,16},{1,21},{... | collective-permute-start | bytes 61448 | tf_op jit(solution)/shard_map/ppermute | solution.py:77
  19.0 5.2 %all_gather.29 = bf16[1,32,64]{2,1,0:T(8,128)(2,1)S(1)} all-gather(bf16[1,8,64]{2,1,0:T(8,128)(2,1)S(1)} %reshape.388), channel_id=1, replica_groups=mesh['sp'=8,'tp'=4] {'tp'}, dimensions={1}, use_global_device_ids=true | all-gather | bytes 5120 | tf_op jit(solution)/shard_map/all_gather | solution.py:117
  24.2 1.8 %fusion.18 = bf16[8,1,512]{2,1,0:T(2,128)(2,1)S(1)} fusion(bf16[1,1024]{1,0:T(2,128)(2,1)} %param.20, bf16[512,1024]{1,0:T(8,128)(2,1)} %param.16), kind=kOutput, calls=%fused_computation.29 | convolution fusion | flops 1048576 | bytes 1058816 | tf_op jit(solution)/shard_map/shd,khd->shk/dot_general | solution.py:112
  25.9 5.2 %all-gather = bf16[32,512]{1,0:T(8,128)(2,1)S(1)} all-gather(bf16[8,512]{1,0:T(8,128)(2,1)S(1)} %bitcast.185), channel_id=2, replica_groups=mesh['sp'=8,'tp'=4] {'tp'}, dimensions={0}, use_global_device_ids=true | all-gather | bytes 40960 | tf_op jit(solution)/shard_map/all_gather | solution.py:116
  31.1 6.1 %fusion.11 = f32[32,8192]{1,0:T(8,128)S(1)} fusion(bf16[32,512]{1,0:T(8,128)(2,1)S(1)} %all-gather, bf16[1,8192,512]{2,1,0:T(8,128)(2,1)} %param.18), kind=kOutput, calls=%fused_computation.18 | convolution fusion | flops 268435456 | bytes 9469952 | tf_op jit(solution)/shard_map/shk,spk->shp/dot_general | solution.py:119
  38.0 1.6 %fusion.9 = f32[32,512]{1,0:T(8,128)S(1)} fusion(bf16[1,8192,512]{2,1,0:T(8,128)(2,1)S(1)} %bitcast.180, f32[32,8192]{1,0:T(8,128)S(1)} %get-tuple-element.238, f32[32]{0:T(128)S(1)} %get-tuple-element.237), kind=kOutput, calls=%fused_computation.16 | convolution fusion | flops 268959744 | bytes 9502848 | tf_op jit(solution)/shard_map/shp,spk->shk/dot_general | solution.py:129
  41.4 7.1 %all-reduce.2 = (f32[128]{0:T(128)S(1)}, f32[128]{0:T(128)S(1)}) all-reduce(f32[128]{0:T(128)S(1)} %dynamic-update-slice, f32[128]{0:T(128)S(1)} %dynamic-update-slice.1), channel_id=3, replica_groups=mesh['sp'=8,'tp'=4] {'tp'}, use_global_device_ids=true, to_apply=%add | all-reduce | flops 256 | bytes 2048
  51.6 5.8 %all-gather.3 = f32[128,512]{1,0:T(8,128)S(1)} all-gather(f32[32,512]{1,0:T(8,128)S(1)} %fusion.9), channel_id=5, replica_groups=mesh['sp'=8,'tp'=4] {'tp'}, dimensions={0}, use_global_device_ids=true | all-gather | bytes 327680 | tf_op jit(solution)/shard_map/all_gather | solution.py:26
  57.4 7.6 %while.19 = (s32[]{:T(128)}, f32[1,32]{1,0:T(1,128)}, f32[1,32]{1,0:T(1,128)}, f32[1,32,512]{2,1,0:T(8,128)S(1)}, f32[4,1,32]{2,1,0:T(1,128)}, /*index=5*/f32[4,...) while((s32[]{:T(128)}, f32[1,32]{1,0:T(1,128)}, f32[1,32]{1,0:T(1,128)}, ...), condition=%wide.region_4.5_spmd, body=%wide.region_3.4_spmd.sunk | while | flops 49381 | bytes 198675 | solution.py:31
  66.9 1.4 %collective-permute-start.5 = (bf16[1,10,1024]{2,1,0:T(8,128)(2,1)S(1)}, bf16[1,10,1024]{2,1,0:T(8,128)(2,1)S(1)}, u32[]{:S(2)}, u32[]{:S(2)}) collective-permute-start(bf16[1,10,1024]{2,1,0:T(8,128)(2,1)S(1)} %copy.51), channel_id=1, source_target_pairs={{0,24},{4,28},{8,0},{12,4},{16,8},{20,12},{24,16},{28,20},{1,25},{... | collective-permute-start | bytes 61448 | tf_op jit(solution)/shard_map/ppermute | solution.py:77
  68.3 1.4 %bitcast_dynamic-update-slice_fusion.6 = bf16[8,1,10,1024]{3,2,1,0:T(8,128)(2,1)} fusion(bf16[8,1,10,1024]{3,2,1,0:T(8,128)(2,1)} %fusion.35, bf16[1,10,1024]{2,1,0:T(8,128)(2,1)} %collective-permute-done), kind=kLoop, calls=%fused_computation.57 | loop fusion | bytes 65536
  69.7 1.4 %collective-permute-start.6 = (bf16[1,10,1024]{2,1,0:T(8,128)(2,1)S(1)}, bf16[1,10,1024]{2,1,0:T(8,128)(2,1)S(1)}, u32[]{:S(2)}, u32[]{:S(2)}) collective-permute-start(bf16[1,10,1024]{2,1,0:T(8,128)(2,1)S(1)} %copy.52), channel_id=1, source_target_pairs={{0,28},{4,0},{8,4},{12,8},{16,12},{20,16},{24,20},{28,24},{1,29},{... | collective-permute-start | bytes 61448 | tf_op jit(solution)/shard_map/ppermute | solution.py:77
  71.1 1.4 %bitcast_dynamic-update-slice_fusion.5 = bf16[8,1,10,1024]{3,2,1,0:T(8,128)(2,1)} fusion(bf16[8,1,10,1024]{3,2,1,0:T(8,128)(2,1)} %bitcast_dynamic-update-slice_fusion.6, bf16[1,10,1024]{2,1,0:T(8,128)(2,1)} %collective-permute-done.1), kind=kLoop, calls=%fused_computation.56 | loop fusion | bytes 65536
  72.5 1.4 %bitcast_dynamic-update-slice_fusion.4 = bf16[8,1,10,1024]{3,2,1,0:T(8,128)(2,1)} fusion(bf16[8,1,10,1024]{3,2,1,0:T(8,128)(2,1)} %bitcast_dynamic-update-slice_fusion.5, bf16[1,10,1024]{2,1,0:T(8,128)(2,1)} %collective-permute-done.2), kind=kLoop, calls=%fused_computation.55 | loop fusion | bytes 65536
  73.9 1.4 %bitcast_dynamic-update-slice_fusion.3 = bf16[8,1,10,1024]{3,2,1,0:T(8,128)(2,1)} fusion(bf16[8,1,10,1024]{3,2,1,0:T(8,128)(2,1)} %bitcast_dynamic-update-slice_fusion.4, bf16[1,10,1024]{2,1,0:T(8,128)(2,1)} %collective-permute-done.3), kind=kLoop, calls=%fused_computation.54 | loop fusion | bytes 65536
  75.3 1.4 %bitcast_dynamic-update-slice_fusion.2 = bf16[8,1,10,1024]{3,2,1,0:T(8,128)(2,1)} fusion(bf16[8,1,10,1024]{3,2,1,0:T(8,128)(2,1)} %bitcast_dynamic-update-slice_fusion.3, bf16[1,10,1024]{2,1,0:T(8,128)(2,1)} %collective-permute-done.4), kind=kLoop, calls=%fused_computation.53 | loop fusion | bytes 65536
  77.9 1.6 %gather_fusion = bf16[8,10,1024]{2,1,0:T(8,128)(2,1)S(1)} fusion(bf16[8,10,1024]{2,1,0:T(8,128)(2,1)} %bitcast.182, s32[1024]{0:T(1024)} %pad_clamp_fusion), kind=kCustom, calls=%fused_computation | custom fusion | bytes 327712 | tf_op jit(solution)/shard_map/gather | solution.py:78
  80.2 7.6 %all_gather.27 = bf16[1,80,4096]{2,1,0:T(8,128)(2,1)S(1)} all-gather(bf16[1,80,1024]{2,1,0:T(8,128)(2,1)} %reshape_transpose.3), channel_id=1, replica_groups=mesh['sp'=8,'tp'=4] {'tp'}, dimensions={2}, use_global_device_ids=true | all-gather | bytes 819200 | tf_op jit(solution)/shard_map/all_gather | solution.py:85
  87.9 1.4 %convolution_bitcast_fusion = f32[1,80,64]{1,2,0:T(8,128)S(1)} fusion(bf16[4096,64]{0,1:T(8,128)(2,1)} %param.14, bf16[1,80,4096]{2,1,0:T(8,128)(2,1)S(1)} %all_gather.27), kind=kOutput, calls=%fused_computation.22 | convolution fusion | flops 41943040 | bytes 1200128 | tf_op jit(solution)/shard_map/dot_general | solution.py:89
  89.3 3.1 %multiply_reduce_fusion = (f32[80]{0:T(128)S(1)}, f32[80,512]{1,0:T(8,128)S(1)}) fusion(bf16[4096,512]{1,0:T(8,128)(2,1)} %param.13, bf16[1,80,4096]{2,1,0:T(8,128)(2,1)S(1)} %all_gather.27), kind=kOutput, calls=%fused_computation.47 | convolution fusion | flops 335626176 | bytes 5013824 | tf_op jit(solution)/shard_map/dot_general | solution.py:88
  (98 shorter events, 26.1 us)
Async XLA Ops:
  0.6 36.6 %copy-start = (bf16[1,8192,64]{1,2,0:T(8,128)(2,1)S(1)}, bf16[1,8192,64]{1,2,0:T(8,128)(2,1)}, u32[]{:S(2)}) copy-start(bf16[1,8192,64]{1,2,0:T(8,128)(2,1)} %param.19) | copy-start | bytes 3145732
  3.6 63.3 %collective-permute-start = (bf16[1,10,1024]{2,1,0:T(8,128)(2,1)}, bf16[1,10,1024]{2,1,0:T(8,128)(2,1)}, u32[]{:S(2)}, u32[]{:S(2)}) collective-permute-start(bf16[1,10,1024]{2,1,0:T(8,128)(2,1)} %copy.46), channel_id=1, source_target_pairs={{0,4},{4,8},{8,12},{12,16},{16,20},{20,24},{24,28},{28,0},{1,5},{5... | collective-permute-start | bytes 61448 | tf_op jit(solution)/shard_map/ppermute | solution.py:77
  7.2 62.5 %collective-permute-start.1 = (bf16[1,10,1024]{2,1,0:T(8,128)(2,1)}, bf16[1,10,1024]{2,1,0:T(8,128)(2,1)}, u32[]{:S(2)}, u32[]{:S(2)}) collective-permute-start(bf16[1,10,1024]{2,1,0:T(8,128)(2,1)} %copy.47), channel_id=1, source_target_pairs={{0,8},{4,12},{8,16},{12,20},{16,24},{20,28},{24,0},{28,4},{1,9},{5... | collective-permute-start | bytes 61448 | tf_op jit(solution)/shard_map/ppermute | solution.py:77
  9.4 63.1 %collective-permute-start.2 = (bf16[1,10,1024]{2,1,0:T(8,128)(2,1)}, bf16[1,10,1024]{2,1,0:T(8,128)(2,1)}, u32[]{:S(2)}, u32[]{:S(2)}) collective-permute-start(bf16[1,10,1024]{2,1,0:T(8,128)(2,1)} %copy.48), channel_id=1, source_target_pairs={{0,12},{4,16},{8,20},{12,24},{16,28},{20,0},{24,4},{28,8},{1,13},{... | collective-permute-start | bytes 61448 | tf_op jit(solution)/shard_map/ppermute | solution.py:77
  12.6 61.3 %collective-permute-start.3 = (bf16[1,10,1024]{2,1,0:T(8,128)(2,1)}, bf16[1,10,1024]{2,1,0:T(8,128)(2,1)}, u32[]{:S(2)}, u32[]{:S(2)}) collective-permute-start(bf16[1,10,1024]{2,1,0:T(8,128)(2,1)} %copy.49), channel_id=1, source_target_pairs={{0,16},{4,20},{8,24},{12,28},{16,0},{20,4},{24,8},{28,12},{1,17},{... | collective-permute-start | bytes 61448 | tf_op jit(solution)/shard_map/ppermute | solution.py:77
  14.4 60.8 %collective-permute-start.4 = (bf16[1,10,1024]{2,1,0:T(8,128)(2,1)}, bf16[1,10,1024]{2,1,0:T(8,128)(2,1)}, u32[]{:S(2)}, u32[]{:S(2)}) collective-permute-start(bf16[1,10,1024]{2,1,0:T(8,128)(2,1)} %copy.50), channel_id=1, source_target_pairs={{0,20},{4,24},{8,28},{12,0},{16,4},{20,8},{24,12},{28,16},{1,21},{... | collective-permute-start | bytes 61448 | tf_op jit(solution)/shard_map/ppermute | solution.py:77
  18.4 0.6 copy-start.7
  24.2 13.8 %slice-start = ((s8[8388608]{0:T(1024)(128)(4,1)}), s8[4194304]{0:T(1024)(128)(4,1)S(1)}, s32[]{:S(2)}) async-start(s8[8388608]{0:T(1024)(128)(4,1)} %bitcast.179), calls=%async_computation | async-start | bytes 8388608
  31.1 6.8 %slice-start.1 = ((s8[8388608]{0:T(1024)(128)(4,1)}), s8[4194304]{0:T(1024)(128)(4,1)S(1)}, s32[]{:S(2)}) async-start(s8[8388608]{0:T(1024)(128)(4,1)} %bitcast.179), calls=%async_computation.1 | async-start | bytes 8388608
  38.0 1.7 %copy-start.13 = (u32[32]{0:T(128)S(1)}, u32[32]{0:T(128)}, u32[]{:S(2)}) copy-start(u32[32]{0:T(128)} %constant.148) | copy-start | bytes 388
  39.6 52.8 %copy-start.1 = (bf16[512,1024]{1,0:T(8,128)(2,1)S(1)}, bf16[512,1024]{1,0:T(8,128)(2,1)}, u32[]{:S(2)}) copy-start(bf16[512,1024]{1,0:T(8,128)(2,1)} %param.16) | copy-start | bytes 3145732
  39.6 53.2 %copy-start.2 = (bf16[512,1024]{1,0:T(8,128)(2,1)S(1)}, bf16[512,1024]{1,0:T(8,128)(2,1)}, u32[]{:S(2)}) copy-start(bf16[512,1024]{1,0:T(8,128)(2,1)} %param.17) | copy-start | bytes 3145732
  66.8 25.6 %copy-start.8 = (f32[512]{0:T(512)S(1)}, f32[512]{0:T(512)}, u32[]{:S(2)}) copy-start(f32[512]{0:T(512)} %param.15) | copy-start | bytes 6148
  66.8 26.3 %copy-start.12 = (bf16[1,1024]{1,0:T(2,128)(2,1)S(1)}, bf16[1,1024]{1,0:T(2,128)(2,1)}, u32[]{:S(2)}) copy-start(bf16[1,1024]{1,0:T(2,128)(2,1)} %param.20) | copy-start | bytes 6148
  66.8 26.5 %copy-start.10 = (f32[80]{0:T(128)S(1)}, f32[80]{0:T(128)}, u32[]{:S(2)}) copy-start(f32[80]{0:T(128)} %add_convert_fusion) | copy-start | bytes 964
  66.9 26.5 %copy-start.11 = (f32[32]{0:T(128)S(1)}, f32[32]{0:T(128)}, u32[]{:S(2)}) copy-start(f32[32]{0:T(128)} %multiply_power_fusion) | copy-start | bytes 388
  66.9 27.3 %copy-start.9 = (bf16[8,64]{1,0:T(8,128)(2,1)S(1)}, bf16[8,64]{1,0:T(8,128)(2,1)}, u32[]{:S(2)}) copy-start(bf16[8,64]{1,0:T(8,128)(2,1)} %reshape.392) | copy-start | bytes 3076
  66.9 27.5 %copy-start.5 = (f32[1,32]{1,0:T(1,128)S(1)}, f32[1,32]{1,0:T(1,128)}, u32[]{:S(2)}) copy-start(f32[1,32]{1,0:T(1,128)} %get-tuple-element.183) | copy-start | bytes 388
  66.9 27.8 %copy-start.6 = (f32[1,32]{1,0:T(1,128)S(1)}, f32[1,32]{1,0:T(1,128)}, u32[]{:S(2)}) copy-start(f32[1,32]{1,0:T(1,128)} %get-tuple-element.184) | copy-start | bytes 388
  66.9 9.7 %collective-permute-start.5 = (bf16[1,10,1024]{2,1,0:T(8,128)(2,1)S(1)}, bf16[1,10,1024]{2,1,0:T(8,128)(2,1)S(1)}, u32[]{:S(2)}, u32[]{:S(2)}) collective-permute-start(bf16[1,10,1024]{2,1,0:T(8,128)(2,1)S(1)} %copy.51), channel_id=1, source_target_pairs={{0,24},{4,28},{8,0},{12,4},{16,8},{20,12},{24,16},{28,20},{1,25},{... | collective-permute-start | bytes 61448 | tf_op jit(solution)/shard_map/ppermute | solution.py:77
  69.7 7.6 %collective-permute-start.6 = (bf16[1,10,1024]{2,1,0:T(8,128)(2,1)S(1)}, bf16[1,10,1024]{2,1,0:T(8,128)(2,1)S(1)}, u32[]{:S(2)}, u32[]{:S(2)}) collective-permute-start(bf16[1,10,1024]{2,1,0:T(8,128)(2,1)S(1)} %copy.52), channel_id=1, source_target_pairs={{0,28},{4,0},{8,4},{12,8},{16,12},{20,16},{24,20},{28,24},{1,29},{... | collective-permute-start | bytes 61448 | tf_op jit(solution)/shard_map/ppermute | solution.py:77
  92.8 3.2 %copy-start.3 = (bf16[80,1024]{1,0:T(8,128)(2,1)}, bf16[80,1024]{1,0:T(8,128)(2,1)S(1)}, u32[]{:S(2)}) copy-start(bf16[80,1024]{1,0:T(8,128)(2,1)S(1)} %convolution_convert_fusion.1) | copy-start | bytes 491524
  93.2 2.8 %copy-start.4 = (bf16[80,1024]{1,0:T(8,128)(2,1)}, bf16[80,1024]{1,0:T(8,128)(2,1)S(1)}, u32[]{:S(2)}) copy-start(bf16[80,1024]{1,0:T(8,128)(2,1)S(1)} %convolution_convert_fusion) | copy-start | bytes 491524
